TPU v7x, 32 devices: a whole 2x2x4 slice. The times are simulated.
32 devices in a mesh: sp: 8 (over z, core), tp: 4 (over y, x).
Axes of the slice: x: 2, y: 2, z: 4, core: 2. Of those that a mesh axis runs over, the one named last changes fastest.
Arguments:
- layer_input: bfloat16 [8192, 4096], P('sp', 'tp'), may hold values from -6 to 6
- key_weight: bfloat16 [4096, 4096], P(None, 'tp'), may hold values from -0.09375 to 0.09375
- value_weight: bfloat16 [4096, 4096], P(None, 'tp'), may hold values from -0.09375 to 0.09375
- decay_exponent: float32 [32], P('tp'), may hold values from -0.077 to -0.00016845703, as said below
- query_new: bfloat16 [2, 4096], P(None, 'tp'), may hold values from -6 to 6
- key_new: bfloat16 [2, 4096], P(None, 'tp'), may hold values from -6 to 6
- value_new: bfloat16 [2, 4096], P(None, 'tp'), may hold values from -6 to 6
- norm_gain: float32 [4096], P('tp'), may hold values from 0.1 to 1.9
Outputs:
- state_cache: bfloat16 [2, 32, 128, 128], P(None, 'tp', 'sp')
- first_read: bfloat16 [2, 4096], P(None, 'tp')
Inputs may be any that keep to these rules, and one draw needn't show every extreme that they name: decay_exponent is negative.
All inputs are finite; a program needn't handle non-finite values.
Results may differ from a plain program's by a relative error of at most 0.011.
Values may be sent and summed in bfloat16 or wider, within the bound.
A program may use at most 64 MiB of HBM per device.

v0:
```python
import jax
import jax.numpy as jnp
from jax import lax
from jax.sharding import PartitionSpec as P

SEQS = 2


def rotate(projected, position):
    half_width = projected.shape[-1] // 2
    inverse = 1.0 / 10000.0 ** jnp.linspace(0.0, 1.0, half_width, dtype=jnp.float32)
    angle = position[:, None] * inverse[None, :]
    cosine = jnp.cos(angle)[:, None, :]
    sine = jnp.sin(angle)[:, None, :]
    first = projected[..., :half_width]
    second = projected[..., half_width:]
    return jnp.concatenate(
        [first * cosine - second * sine, first * sine + second * cosine], axis=-1
    )


def on_device(
    layer_input, key_weight, value_weight, decay_exponent, query_new, key_new, value_new, norm_gain
):
    tok_count = layer_input.shape[0]
    head_local = decay_exponent.shape[0]
    key_width = key_weight.shape[1] // head_local
    value_width = value_weight.shape[1] // head_local
    seq_span = lax.axis_size("sp") // SEQS
    seq_length = tok_count * seq_span
    sp_place = lax.axis_index("sp")
    feature_block = lax.all_gather(layer_input, "tp", axis=1, tiled=True)
    key_proj = jnp.dot(feature_block, key_weight, preferred_element_type=jnp.float32)
    value_proj = jnp.dot(feature_block, value_weight, preferred_element_type=jnp.float32)
    position = (sp_place % seq_span * tok_count + jnp.arange(tok_count, dtype=jnp.int32)).astype(
        jnp.float32
    )
    keys = (
        rotate(key_proj.reshape(tok_count, head_local, key_width), position) * key_width ** (-0.5)
    ).astype(jnp.bfloat16)
    values = value_proj.astype(jnp.bfloat16).reshape(tok_count, head_local, value_width)
    distance = seq_length - 1.0 - position
    weighting = jnp.exp(decay_exponent[None, :] * distance[:, None])
    weighted = (keys.astype(jnp.float32) * weighting[:, :, None]).astype(jnp.bfloat16)
    local_state = jnp.einsum("thd,the->hde", weighted, values, preferred_element_type=jnp.float32)
    member = (jnp.arange(SEQS, dtype=jnp.int32) == sp_place // seq_span).astype(jnp.float32)
    state_terms = member[:, None, None, None] * local_state[None]
    final_rows = lax.psum_scatter(state_terms, "sp", scatter_dimension=2, tiled=True)
    state_cache = final_rows.astype(jnp.bfloat16)
    queries = query_new.astype(jnp.float32).reshape(SEQS, head_local, key_width)
    partial_read = jnp.einsum(
        "shd,shde->she", queries, state_terms, precision=lax.Precision.HIGHEST
    )
    carried = lax.psum(partial_read, "sp")
    keys_next = key_new.astype(jnp.float32).reshape(SEQS, head_local, key_width)
    values_next = value_new.astype(jnp.float32).reshape(SEQS, head_local, value_width)
    own_term = jnp.sum(queries * keys_next, axis=2)[:, :, None] * values_next
    mixed = jnp.exp(decay_exponent)[None, :, None] * carried + own_term
    normed = mixed * lax.rsqrt(jnp.mean(mixed * mixed, axis=2, keepdims=True) + 1e-06)
    normed = normed * norm_gain.reshape(head_local, value_width)[None, :, :]
    return (state_cache, normed.reshape(SEQS, head_local * value_width).astype(jnp.bfloat16))


def solution(mesh):
    in_specs = (
        P("sp", "tp"),
        P(None, "tp"),
        P(None, "tp"),
        P("tp"),
        P(None, "tp"),
        P(None, "tp"),
        P(None, "tp"),
        P("tp"),
    )
    out_specs = (P(None, "tp", "sp", None), P(None, "tp"))
    return jax.shard_map(
        on_device, mesh=mesh, in_specs=in_specs, out_specs=out_specs, check_vma=False
    )
```

profile of v0, /device:TPU:0, one launch (start us, length us, event | category | flops | bytes accessed | tf_op | source)
XLA Modules:
  0.0 171.2 jit_solution(11473532928308546510)
XLA Ops:
  7.2 0.0 all-gather.2.cloned.1.call-start
  7.2 0.7 all-gather.2.cloned.1.call-update
  7.9 0.0 reduce-scatter.2.cloned.1.call-start
  8.0 0.1 fusion.12
  8.1 0.7 multiply_exponential_fusion
  8.8 1.0 multiply_cosine_fusion
  9.8 90.2 %all-gather.2.cloned.1.call-done = bf16[1024,4096]{1,0:T(8,128)(2,1)} async-done(((bf16[1024,1024]{1,0:T(8,128)(2,1)}), bf16[1024,4096]{1,0:T(8,128)(2,1)}) %all-gather.2.cloned.1.call-update) | async-done | bytes 8388624 | tf_op jit(solution)/shard_map/all_gather | solution.py:32
  100.1 13.2 %fusion.15 = f32[1024,1024]{0,1:T(8,128)S(1)} fusion(bf16[1024,4096]{1,0:T(8,128)(2,1)} %all-gather.2.cloned.1.call-done, bf16[4096,1024]{1,0:T(8,128)(2,1)} %param.9), kind=kOutput, calls=%fused_computation.35 | convolution fusion | flops 8589934592 | bytes 20971520 | tf_op jit(solution)/shard_map/dot_general | solution.py:33
  113.3 1.0 multiply_subtract_fusion
  114.3 13.8 %convolution_convert_fusion = bf16[1024,1024]{0,1:T(8,128)(2,1)S(1)} fusion(bf16[1024,4096]{1,0:T(8,128)(2,1)} %all-gather.2.cloned.1.call-done, bf16[4096,1024]{1,0:T(8,128)(2,1)} %param.10), kind=kOutput, calls=%fused_computation.9 | convolution fusion | flops 8590983168 | bytes 18874368 | tf_op jit(solution)/shard_map/dot_general | solution.py:34
  128.1 0.0 copy-start.4
  128.1 0.0 copy-start
  128.1 0.0 copy-start.1
  128.1 0.0 copy-start.3
  128.1 0.0 copy-start.2
  128.1 0.7 fusion.2
  128.9 1.1 broadcast_multiply_fusion
  130.0 0.0 reduce-scatter.2.cloned.1.call-update
  130.0 0.0 copy-done.4
  130.0 0.0 copy-done
  130.1 0.0 copy-done.1
  130.1 0.0 copy-done.3
  130.1 0.7 fusion.8
  130.8 16.6 %psum.7 = f32[2,8,128]{2,1,0:T(8,128)S(1)} all-reduce(f32[2,8,128]{2,1,0:T(8,128)S(1)} %bitcast.29), channel_id=1, replica_groups=mesh['sp'=8,'tp'=4] {'sp'}, use_global_device_ids=true, to_apply=%region_1.2 | all-reduce | flops 2048 | bytes 16384 | tf_op jit(solution)/shard_map/psum | solution.py:54
  147.4 0.2 multiply_reduce_fusion
  147.6 0.0 copy-done.2
  147.6 0.1 fusion.11
  147.6 0.6 copy.26
  148.2 14.6 %reduce-scatter.2.cloned.1.call-done = f32[2,8,16,128]{3,2,1,0:T(8,128)} async-done(((f32[2,8,128,128]{3,2,1,0:T(8,128)}), f32[2,8,16,128]{3,2,1,0:T(8,128)}) %reduce-scatter.2.cloned.1.call-update) | async-done | bytes 131088 | tf_op jit(solution)/shard_map/reduce_scatter | solution.py:48
  162.8 1.5 convert_element_type.51
  (9 shorter events, 0.1 us)
Async XLA Ops:
  7.2 92.9 %all-gather.2.cloned.1.call-start = ((), (), s32[]{:S(2)}) async-start(), calls=%async_computation.1 | async-start | bytes 10485760 | tf_op jit(solution)/shard_map/all_gather | solution.py:32
  7.9 154.9 %reduce-scatter.2.cloned.1.call-start = ((), (), s32[]{:S(2)}) async-start(), calls=%async_computation.2 | async-start | bytes 1179648 | tf_op jit(solution)/shard_map/reduce_scatter | solution.py:48
  128.1 1.9 %copy-start.4 = (f32[8]{0:T(128)S(1)}, f32[8]{0:T(128)}, u32[]{:S(2)}) copy-start(f32[8]{0:T(128)} %param.11) | copy-start | bytes 100
  128.1 2.0 %copy-start = (bf16[2,1024]{1,0:T(2,128)(2,1)S(1)}, bf16[2,1024]{1,0:T(2,128)(2,1)}, u32[]{:S(2)}) copy-start(bf16[2,1024]{1,0:T(2,128)(2,1)} %param.12) | copy-start | bytes 12292
  128.1 2.0 %copy-start.1 = (bf16[2,1024]{1,0:T(2,128)(2,1)S(1)}, bf16[2,1024]{1,0:T(2,128)(2,1)}, u32[]{:S(2)}) copy-start(bf16[2,1024]{1,0:T(2,128)(2,1)} %param.14) | copy-start | bytes 12292
  128.1 2.0 %copy-start.3 = (bf16[2,1024]{1,0:T(2,128)(2,1)S(1)}, bf16[2,1024]{1,0:T(2,128)(2,1)}, u32[]{:S(2)}) copy-start(bf16[2,1024]{1,0:T(2,128)(2,1)} %param.13) | copy-start | bytes 12292
  128.1 19.4 %copy-start.2 = (f32[1024]{0:T(1024)S(1)}, f32[1024]{0:T(1024)}, u32[]{:S(2)}) copy-start(f32[1024]{0:T(1024)} %param.15) | copy-start | bytes 12292
Sparse Core Ops, SparseCore 0:
  9.8 90.1 all-gather.1
  130.1 32.6 reduce-scatter.1
where the time goes:
time: 171 us
  waiting for transfers between devices  106 us (62%)
  matrix products  28.4 us (17%)
  blocking collectives  16.6 us (10%)
  between operations  14.2 us (8%)
  other arithmetic  5.78 us (3%)
    all_gather x1, waiting for transfers between devices, on_device(): feature_block = lax.all_gather(layer_input, 'tp', axis=1, tiled=True)  90.2 us
    psum x1, blocking collectives, on_device(): carried = lax.psum(partial_read, 'sp')  16.6 us
    reduce_scatter x1, waiting for transfers between devices, on_device(): lax.psum_scatter(state_terms, 'sp', scatter_dimension=2, tiled=True)  14.6 us
    dot_general x1, matrix products, on_device(): jnp.dot(feature_block, value_weight, preferred_element_type=jnp.float32)  13.8 us
    dot_general x1, matrix products, on_device(): jnp.dot(feature_block, key_weight, preferred_element_type=jnp.float32)  13.2 us
  transfers between devices with their start and end apart: 2, of which 2 were waited for; matrix products, arithmetic and copies ran while one was open for 2% of the time, Pallas kernels for 0%

commit v1 on v0

--- a/solution.py
+++ b/solution.py
@@ -29,7 +29,7 @@
     seq_span = lax.axis_size("sp") // SEQS
     seq_length = tok_count * seq_span
     sp_place = lax.axis_index("sp")
-    feature_block = lax.all_gather(layer_input, "tp", axis=1, tiled=True)
+    feature_block = jnp.concatenate(lax.all_gather(layer_input, "tp"), axis=1)
     key_proj = jnp.dot(feature_block, key_weight, preferred_element_type=jnp.float32)
     value_proj = jnp.dot(feature_block, value_weight, preferred_element_type=jnp.float32)
     position = (sp_place % seq_span * tok_count + jnp.arange(tok_count, dtype=jnp.int32)).astype(

time: 171 us -> 211 us (1.23)
  local copies, waits for them, and re-layouts: 0.65 us -> 52 us
  waiting for transfers between devices: 106 us -> 94.6 us
    reshape x0 -> x1, local copies, waits for them, and re-layouts: none -> 14.5 us  [on_device(): feature_block = jnp.concatenate(lax.all_gather(layer_input, 'tp'), axis=1)]
    unnamed x11 -> x16, local copies, waits for them, and re-layouts: 0.64 us -> 13.6 us
    all_gather x0 -> x1, local copies, waits for them, and re-layouts: none -> 12.1 us  [on_device(): feature_block = jnp.concatenate(lax.all_gather(layer_input, 'tp'), axis=1)]
    dot_general x0 -> x1, local copies, waits for them, and re-layouts: none -> 11.8 us  [on_device(): jnp.dot(feature_block, key_weight, preferred_element_type=jnp.float32)]
    all_gather x1, waiting for transfers between devices: 90.2 us -> 79.1 us  [on_device(): feature_block = jnp.concatenate(lax.all_gather(layer_input, 'tp'), axis=1)]
  transfers between devices with their start and end apart: 2 -> 2, of which waited for: 2 -> 2; matrix products, arithmetic and copies ran while one was open for 2% -> 7% of each run, Pallas kernels for 0% -> 0%
where the time goes in v1:
time: 211 us; the launch traced here: 210 us
  waiting for transfers between devices  94.6 us (45%)
  local copies, waits for them, and re-layouts  52 us (25%)
  matrix products  28 us (13%)
  blocking collectives  16.5 us (8%)
  between operations  14.2 us (7%)
  other arithmetic  4.85 us (2%)
    all_gather x1, waiting for transfers between devices, on_device(): feature_block = jnp.concatenate(lax.all_gather(layer_input, 'tp'), axis=1)  79.1 us
    psum x1, blocking collectives, on_device(): carried = lax.psum(partial_read, 'sp')  16.5 us
    reduce_scatter x1, waiting for transfers between devices, on_device(): lax.psum_scatter(state_terms, 'sp', scatter_dimension=2, tiled=True)  14.8 us
    dot_general x1, matrix products, on_device(): jnp.dot(feature_block, value_weight, preferred_element_type=jnp.float32)  14.8 us
    reshape x1, local copies, waits for them, and re-layouts, on_device(): feature_block = jnp.concatenate(lax.all_gather(layer_input, 'tp'), axis=1)  14.5 us
    unnamed x16, local copies, waits for them, and re-layouts  13.6 us
    all_gather x1, local copies, waits for them, and re-layouts, on_device(): feature_block = jnp.concatenate(lax.all_gather(layer_input, 'tp'), axis=1)  12.1 us
    dot_general x1, local copies, waits for them, and re-layouts, on_device(): jnp.dot(feature_block, key_weight, preferred_element_type=jnp.float32)  11.8 us
  transfers between devices with their start and end apart: 2, of which 2 were waited for; matrix products, arithmetic and copies ran while one was open for 7% of the time, Pallas kernels for 0%

profile of v1, /device:TPU:0, one launch (start us, length us, event | category | flops | bytes accessed | tf_op | source)
XLA Modules:
  0.0 210.3 jit_solution(13932825409182763878)
XLA Ops:
  7.2 0.0 all-gather.3.cloned.1.call-start
  7.2 0.7 all-gather.3.cloned.1.call-update
  7.9 0.0 reduce-scatter.2.cloned.1.call-start
  8.0 0.0 copy-start.5
  8.0 11.8 %copy.16 = bf16[1024,4096]{1,0:T(8,128)(2,1)} copy(bf16[1024,4096]{0,1:T(8,128)(2,1)} %bitcast.37) | data formatting | bytes 16777216 | tf_op jit(solution)/shard_map/dot_general | solution.py:33
  19.8 0.1 fusion.12
  19.9 0.0 copy-done.5
  19.9 0.1 multiply_exponential_fusion
  20.0 1.0 multiply_cosine_fusion
  21.0 79.1 %all-gather.3.cloned.1.call-done = bf16[4096,1024]{1,0:T(8,128)(2,1)} async-done(((bf16[1024,1024]{1,0:T(8,128)(2,1)}), bf16[4096,1024]{1,0:T(8,128)(2,1)}) %all-gather.3.cloned.1.call-update) | async-done | bytes 8388624 | tf_op jit(solution)/shard_map/all_gather | solution.py:32
  100.1 12.1 %copy.33 = bf16[4,1024,1024]{2,0,1:T(4,128)(2,1)} copy(bf16[4,1024,1024]{2,1,0:T(8,128)(2,1)} %bitcast.38) | data formatting | bytes 16777216 | tf_op jit(solution)/shard_map/all_gather | solution.py:32
  112.2 12.1 %copy.17 = bf16[128,8,4,1024]{3,1,2,0:T(8,128)(2,1)} copy(bf16[128,8,4,1024]{3,2,1,0:T(4,128)(2,1)} %bitcast.35) | data formatting | bytes 16777216
  124.3 14.5 %reshape.157 = bf16[1024,4096,1]{1,0,2:T(8,128)(2,1)} reshape(bf16[1024,4,1024]{2,1,0:T(4,128)(2,1)} %bitcast.36) | data formatting | bytes 16777216 | tf_op jit(solution)/shard_map/reshape | solution.py:32
  138.8 0.0 copy-start
  138.8 14.8 %convolution_convert_fusion = bf16[1024,1024]{0,1:T(8,128)(2,1)} fusion(bf16[1024,4096]{1,0:T(8,128)(2,1)} %bitcast.40, bf16[4096,1024]{1,0:T(8,128)(2,1)} %param.10), kind=kOutput, calls=%fused_computation.9 | convolution fusion | flops 8590983168 | bytes 18874368 | tf_op jit(solution)/shard_map/dot_general | solution.py:34
  153.6 0.0 copy-done
  153.6 11.7 %fusion.15 = f32[1024,8,128]{0,2,1:T(8,128)S(1)} fusion(bf16[1024,4096,1]{1,0,2:T(8,128)(2,1)S(1)} %copy-done, bf16[8,128,4096]{2,1,0:T(8,128)(2,1)} %bitcast.39), kind=kOutput, calls=%fused_computation.36 | convolution fusion | flops 8589934592 | bytes 20971520 | tf_op jit(solution)/shard_map/dot_general | solution.py:33
  165.3 0.0 copy-start.6
  165.3 0.7 multiply_subtract_fusion
  166.1 0.8 copy-done.6
  166.9 0.0 copy-start.1
  166.9 0.0 copy-start.2
  166.9 0.0 copy-start.4
  166.9 0.0 copy-start.3
  166.9 0.8 fusion.2
  167.7 1.2 broadcast_multiply_fusion
  168.9 0.0 reduce-scatter.2.cloned.1.call-update
  168.9 0.0 copy-done.1
  168.9 0.0 copy-done.2
  169.0 0.0 copy-done.4
  169.0 0.7 fusion.8
  169.7 16.5 %psum.7 = f32[2,8,128]{2,1,0:T(8,128)S(1)} all-reduce(f32[2,8,128]{2,1,0:T(8,128)S(1)} %bitcast.41), channel_id=1, replica_groups=mesh['sp'=8,'tp'=4] {'sp'}, use_global_device_ids=true, to_apply=%region_1.2 | all-reduce | flops 2048 | bytes 16384 | tf_op jit(solution)/shard_map/psum | solution.py:54
  186.2 0.2 multiply_reduce_fusion
  186.4 0.0 copy-done.3
  186.4 0.1 fusion.11
  186.4 0.6 copy.32
  187.1 14.8 %reduce-scatter.2.cloned.1.call-done = f32[2,8,16,128]{3,2,1,0:T(8,128)} async-done(((f32[2,8,128,128]{3,2,1,0:T(8,128)}), f32[2,8,16,128]{3,2,1,0:T(8,128)}) %reduce-scatter.2.cloned.1.call-update) | async-done | bytes 131088 | tf_op jit(solution)/shard_map/reduce_scatter | solution.py:48
  201.9 1.5 convert_element_type.51
  (9 shorter events, 0.1 us)
Async XLA Ops:
  7.2 92.9 %all-gather.3.cloned.1.call-start = ((), (), s32[]{:S(2)}) async-start(), calls=%async_computation.2 | async-start | bytes 10485760 | tf_op jit(solution)/shard_map/all_gather | solution.py:32
  7.9 194.0 %reduce-scatter.2.cloned.1.call-start = ((), (), s32[]{:S(2)}) async-start(), calls=%async_computation.1 | async-start | bytes 1179648 | tf_op jit(solution)/shard_map/reduce_scatter | solution.py:48
  8.0 11.9 %copy-start.5 = (f32[8]{0:T(128)S(1)}, f32[8]{0:T(128)}, u32[]{:S(2)}) copy-start(f32[8]{0:T(128)} %param.11) | copy-start | bytes 100
  138.8 14.8 %copy-start = (bf16[1024,4096,1]{1,0,2:T(8,128)(2,1)S(1)}, bf16[1024,4096,1]{1,0,2:T(8,128)(2,1)}, u32[]{:S(2)}) copy-start(bf16[1024,4096,1]{1,0,2:T(8,128)(2,1)} %reshape.157) | copy-start | bytes 25165828
  165.3 1.6 copy-start.6
  166.9 2.0 copy-start.1
  166.9 2.0 copy-start.2
  166.9 2.1 copy-start.4
  166.9 19.5 %copy-start.3 = (f32[1024]{0:T(1024)S(1)}, f32[1024]{0:T(1024)}, u32[]{:S(2)}) copy-start(f32[1024]{0:T(1024)} %param.15) | copy-start | bytes 12292
Sparse Core Ops, SparseCore 0:
  9.8 90.1 all-gather.2
  169.0 32.8 reduce-scatter.1
